TPU v7x, 256 devices: a whole 4x4x8 slice. The times are simulated.
256 devices in a mesh: fs: 32 (over z, x), tp: 8 (over y, core).
Axes of the slice: x: 4, y: 4, z: 8, core: 2. Of those that a mesh axis runs over, the one named last changes fastest.
Arguments:
- tokens: bfloat16 [16384, 2048], P('fs', 'tp'), may hold values from -6 to 6
- pre_gain: float32 [2048], replicated, may hold values from 0.1 to 1.9
- pre_gate: float32 [2048, 2816], P('fs', 'tp'), may hold values from -0.125 to 0.125
- pre_up: float32 [2048, 2816], P('fs', 'tp'), may hold values from -0.125 to 0.125
- pre_down: float32 [2816, 2048], P('fs', 'tp'), may hold values from -0.109375 to 0.109375
- mix_gain: float32 [2048], replicated, may hold values from 0.1 to 1.9
- branch_proj: float32 [2048, 1024], P('fs', 'tp'), may hold values from -0.125 to 0.125
- gate_proj: float32 [2048, 1024], P('fs', 'tp'), may hold values from -0.125 to 0.125
- conv_taps: float32 [4, 1024], P(None, 'tp'), may hold values from -3 to 3
- retain_blocks: float32 [16, 64, 64], P('tp'), may hold values from -0.75 to 0.75
- admit_blocks: float32 [16, 64, 64], P('tp'), may hold values from -0.75 to 0.75
- decay_param: float32 [1024], P('tp'), may hold values from 5 to 8.5
- channel_gain: float32 [1024], replicated, may hold values from 0.1 to 1.9
- out_proj: float32 [1024, 2048], P('fs', 'tp'), may hold values from -0.1875 to 0.1875
- post_gain: float32 [2048], replicated, may hold values from 0.1 to 1.9
- post_gate: float32 [2048, 2816], P('fs', 'tp'), may hold values from -0.125 to 0.125
- post_up: float32 [2048, 2816], P('fs', 'tp'), may hold values from -0.125 to 0.125
- post_down: float32 [2816, 2048], P('fs', 'tp'), may hold values from -0.109375 to 0.109375
Outputs:
- layer_out: bfloat16 [16384, 2048], P('fs', 'tp')
All inputs are finite; a program needn't handle non-finite values.
Results may differ from a plain program's by a relative error of at most 0.012.
Values may be sent and summed in bfloat16 or wider, within the bound.
A program may use at most 64 MiB of HBM per device.

v0:
```python
import jax
import jax.numpy as jnp
from jax import lax
from jax.sharding import Mesh
from jax.sharding import PartitionSpec as P

SEQ_LEN = 128
FS = ("fs_0", "fs_1")
EPSILON = 1e-06
DECAY_SCALE = 8.0


def copy_for_each(x, axis):
    copies = jnp.broadcast_to(x, (lax.axis_size(axis), *x.shape))
    return lax.all_to_all(copies, axis, split_axis=0, concat_axis=0, tiled=True)


def laid_out(parts, dim):
    dims = list(parts.shape[1:])
    dims[dim] *= parts.shape[0]
    return jnp.moveaxis(parts, 0, dim).reshape(dims)


def gather_directly(x, axis, dim):
    parts = copy_for_each(x, axis)
    return laid_out(parts, dim)


def gathered_by_axis(x, axes, dim):
    whole = x
    for number in range(len(axes) - 1, -1, -1):
        whole = lax.all_gather(whole, axes[number], axis=dim, tiled=True)
    return whole


def normalize(values, norm_gain):
    floats = values.astype(jnp.float32)
    scaled = floats * lax.rsqrt(jnp.mean(floats * floats, axis=-1, keepdims=True) + EPSILON)
    return (scaled * norm_gain).astype(jnp.bfloat16)


def combine(earlier, latter):
    keep_early, add_early = earlier
    keep_late, add_late = latter
    return (keep_early * keep_late, keep_late * add_early + add_late)


def widen(residual):
    return gather_directly(residual, "tp", 1)


def contract(operand, stacked):
    return jnp.dot(
        operand,
        gathered_by_axis(stacked.astype(jnp.bfloat16), FS, 0),
        preferred_element_type=jnp.float32,
    )


def feed_forward(residual, norm_gain, gate_matrix, up_matrix, down_matrix):
    normed = normalize(widen(residual), norm_gain)
    products = contract(normed, jnp.concatenate((gate_matrix, up_matrix), axis=1))
    split_at = gate_matrix.shape[1]
    hidden = (jax.nn.silu(products[:, :split_at]) * products[:, split_at:]).astype(jnp.bfloat16)
    all_hidden = lax.all_gather(hidden, "tp", axis=1, tiled=True)
    return (residual.astype(jnp.float32) + 0.5 * contract(all_hidden, down_matrix)).astype(
        jnp.bfloat16
    )


def block_gate(convolved, blocks):
    grouped = convolved.reshape(
        convolved.shape[0], convolved.shape[1], blocks.shape[0], blocks.shape[1]
    )
    mixed = jnp.einsum(
        "sthi,hij->sthj", grouped, blocks.astype(jnp.bfloat16), preferred_element_type=jnp.float32
    )
    return jax.nn.sigmoid(mixed).reshape(convolved.shape)


def recurrent_mixer(
    residual,
    norm_gain,
    branch_matrix,
    gate_matrix,
    conv_taps,
    retain_blocks,
    admit_blocks,
    decay_param,
    channel_gain,
    out_matrix,
):
    normed = normalize(widen(residual), norm_gain)
    products = contract(normed, jnp.concatenate((branch_matrix, gate_matrix), axis=1))
    local_width = branch_matrix.shape[1]
    branch = products[:, :local_width]
    gate_act = products[:, local_width:]
    taps_count = conv_taps.shape[0]
    sequences = residual.shape[0] // SEQ_LEN
    framed = branch.reshape(sequences, SEQ_LEN, local_width)
    padded = jnp.pad(framed, ((0, 0), (taps_count - 1, 0), (0, 0)))
    convolved = jnp.zeros_like(framed)
    for tap_index in range(taps_count):
        convolved = convolved + padded[:, tap_index : tap_index + SEQ_LEN] * conv_taps[tap_index]
    convolved = convolved.astype(jnp.bfloat16)
    retained = block_gate(convolved, retain_blocks)
    admitted = block_gate(convolved, admit_blocks)
    log_keep = -DECAY_SCALE * retained * jax.nn.softplus(-decay_param)
    inject = jnp.sqrt(-jnp.expm1(2.0 * log_keep)) * admitted * convolved.astype(jnp.float32)
    _, states = lax.associative_scan(combine, (jnp.exp(log_keep), inject), axis=1)
    mixed_rows = (states.reshape(residual.shape[0], local_width) * jax.nn.gelu(gate_act)).astype(
        jnp.bfloat16
    )
    all_channels = gather_directly(mixed_rows, "tp", 1)
    mixed_normed = normalize(all_channels, channel_gain)
    return (residual.astype(jnp.float32) + contract(mixed_normed, out_matrix)).astype(jnp.bfloat16)


def local(
    tokens,
    pre_gain,
    pre_gate,
    pre_up,
    pre_down,
    mix_gain,
    branch_proj,
    gate_proj,
    conv_taps,
    retain_blocks,
    admit_blocks,
    decay_param,
    channel_gain,
    out_proj,
    post_gain,
    post_gate,
    post_up,
    post_down,
):
    after_pre = feed_forward(tokens, pre_gain, pre_gate, pre_up, pre_down)
    after_mix = recurrent_mixer(
        after_pre,
        mix_gain,
        branch_proj,
        gate_proj,
        conv_taps,
        retain_blocks,
        admit_blocks,
        decay_param,
        channel_gain,
        out_proj,
    )
    return feed_forward(after_mix, post_gain, post_gate, post_up, post_down)


def solution(mesh):
    torus = Mesh(mesh.devices.reshape(8, 4, mesh.shape["tp"]), ("fs_0", "fs_1", "tp"))
    placed = (
        P(FS, "tp"),
        P(),
        P(FS, "tp"),
        P(FS, "tp"),
        P(FS, "tp"),
        P(),
        P(FS, "tp"),
        P(FS, "tp"),
        P(None, "tp"),
        P("tp", None, None),
        P("tp", None, None),
        P("tp"),
        P(),
        P(FS, "tp"),
        P(),
        P(FS, "tp"),
        P(FS, "tp"),
        P(FS, "tp"),
    )
    return jax.shard_map(local, mesh=torus, in_specs=placed, out_specs=P(FS, "tp"), check_vma=False)
```

profile of v0, /device:TPU:1, one launch (start us, length us, event | category | flops | bytes accessed | tf_op | source)
XLA Modules:
  0.0 431.4 jit_solution(11646481140543656673)
XLA Ops:
  8.4 12.3 %all_gather.42 = bf16[256,704]{1,0:T(8,128)(2,1)} all-gather(bf16[64,704]{1,0:T(8,128)(2,1)S(1)} %pad_maximum_fusion.3), channel_id=1, replica_groups=mesh['fs_0'=8,'fs_1'=4,'tp'=8] {'fs_1'}, dimensions={0}, use_global_device_ids=true | all-gather | bytes 450560 | tf_op jit(solution)/shard_map/all_gather | solution.py:32
  23.4 8.2 %all-to-all-start = ((bf16[8,512,256]{1,2,0:T(8,128)(2,1)}), bf16[8,512,256]{1,2,0:T(8,128)(2,1)S(1)}, u32[]{:S(2)}, u32[]{:S(2)}) async-start(bf16[8,512,256]{1,2,0:T(8,128)(2,1)} %broadcast_in_dim.8), calls=%async_computation | async-start | bytes 4194304 | tf_op jit(solution)/shard_map/all_to_all | solution.py:15
  31.6 10.6 %all_gather.45 = bf16[352,256]{1,0:T(8,128)(2,1)} all-gather(bf16[88,256]{1,0:T(8,128)(2,1)S(1)} %convert_element_type.124), channel_id=1, replica_groups=mesh['fs_0'=8,'fs_1'=4,'tp'=8] {'fs_1'}, dimensions={0}, use_global_device_ids=true | all-gather | bytes 225280 | tf_op jit(solution)/shard_map/all_gather | solution.py:32
  42.2 15.5 %all-to-all-done = bf16[8,512,256]{1,2,0:T(8,128)(2,1)S(1)} async-done(((bf16[8,512,256]{1,2,0:T(8,128)(2,1)}), bf16[8,512,256]{1,2,0:T(8,128)(2,1)S(1)}, u32[]{:S(2)}, u32[]{:S(2)}) %all-to-all-start) | async-done | bytes 2097184 | tf_op jit(solution)/shard_map/all_to_all | solution.py:15
  60.2 10.1 %all-gather.8.cloned.1.call-done = bf16[2048,704]{1,0:T(8,128)(2,1)} async-done(((bf16[256,704]{1,0:T(8,128)(2,1)}), bf16[2048,704]{1,0:T(8,128)(2,1)}) %all-gather.8.cloned.1.call-update) | async-done | bytes 2883600 | tf_op jit(solution)/shard_map/all_gather | solution.py:32
  70.3 4.2 fusion.56
  75.6 10.4 %all_gather.47 = bf16[256,256]{1,0:T(8,128)(2,1)} all-gather(bf16[64,256]{1,0:T(8,128)(2,1)S(1)} %pad_maximum_fusion.5), channel_id=1, replica_groups=mesh['fs_0'=8,'fs_1'=4,'tp'=8] {'fs_1'}, dimensions={0}, use_global_device_ids=true | all-gather | bytes 163840 | tf_op jit(solution)/shard_map/all_gather | solution.py:32
  86.1 20.4 %all-gather.12.cloned.1.call-done = bf16[2816,256]{1,0:T(8,128)(2,1)} async-done(((bf16[352,256]{1,0:T(8,128)(2,1)}), bf16[2816,256]{1,0:T(8,128)(2,1)}) %all-gather.12.cloned.1.call-update) | async-done | bytes 1441808 | tf_op jit(solution)/shard_map/all_gather | solution.py:32
  106.5 34.1 %all-gather.10.cloned.1.call-done = bf16[512,2816]{0,1:T(8,128)(2,1)} async-done(((bf16[512,352]{0,1:T(8,128)(2,1)}), bf16[512,2816]{0,1:T(8,128)(2,1)}) %all-gather.10.cloned.1.call-update) | async-done | bytes 2883600 | tf_op jit(solution)/shard_map/all_gather | solution.py:65
  140.6 3.2 fusion.12
  145.5 3.9 all-to-all-start.1
  149.5 11.1 %all_gather.51 = bf16[256,704]{1,0:T(8,128)(2,1)} all-gather(bf16[64,704]{1,0:T(8,128)(2,1)S(1)} %pad_maximum_fusion.4), channel_id=1, replica_groups=mesh['fs_0'=8,'fs_1'=4,'tp'=8] {'fs_1'}, dimensions={0}, use_global_device_ids=true | all-gather | bytes 450560 | tf_op jit(solution)/shard_map/all_gather | solution.py:32
  160.7 15.0 %all-to-all-done.1 = bf16[8,512,256]{1,2,0:T(8,128)(2,1)S(1)} async-done(((bf16[8,512,256]{1,2,0:T(8,128)(2,1)}), bf16[8,512,256]{1,2,0:T(8,128)(2,1)S(1)}, u32[]{:S(2)}, u32[]{:S(2)}) %all-to-all-start.1) | async-done | bytes 2097184 | tf_op jit(solution)/shard_map/all_to_all | solution.py:15
  178.0 2.6 fusion.57
  182.9 4.9 %slice.212 = f32[4,64,128]{1,2,0:T(8,128)S(1)} slice(f32[4,128,128]{1,2,0:T(8,128)S(1)} %get-tuple-element.6), slice={[0:4:1], [0:127:2], [0:128:1]} | slice | bytes 262144 | tf_op jit(solution)/shard_map/slice | solution.py:110
  187.9 4.5 %slice.213 = f32[4,64,128]{1,2,0:T(8,128)S(1)} slice(f32[4,128,128]{1,2,0:T(8,128)S(1)} %get-tuple-element.6), slice={[0:4:1], [1:128:2], [0:128:1]} | slice | bytes 262144 | tf_op jit(solution)/shard_map/slice | solution.py:110
  192.4 4.5 %slice.211 = f32[4,64,128]{1,2,0:T(8,128)S(1)} slice(f32[4,128,128]{1,2,0:T(8,128)S(1)} %get-tuple-element.5), slice={[0:4:1], [1:128:2], [0:128:1]} | slice | bytes 262144 | tf_op jit(solution)/shard_map/slice | solution.py:110
  197.0 4.5 %slice.215 = f32[4,64,128]{1,2,0:T(8,128)S(1)} slice(f32[4,128,128]{1,2,0:T(8,128)S(1)} %get-tuple-element.5), slice={[0:4:1], [0:127:2], [0:128:1]} | slice | bytes 262144 | tf_op jit(solution)/shard_map/slice | solution.py:110
  245.6 4.5 %slice.259 = f32[4,63,128]{1,2,0:T(8,128)S(1)} slice(f32[4,128,128]{1,2,0:T(8,128)S(1)} %get-tuple-element.6), slice={[0:4:1], [2:128:2], [0:128:1]} | slice | bytes 258048 | tf_op jit(solution)/shard_map/slice | solution.py:110
  250.1 4.5 %slice.210 = f32[4,63,128]{1,2,0:T(8,128)S(1)} slice(f32[4,128,128]{1,2,0:T(8,128)S(1)} %get-tuple-element.5), slice={[0:4:1], [2:128:2], [0:128:1]} | slice | bytes 258048 | tf_op jit(solution)/shard_map/slice | solution.py:110
  276.4 4.6 %pad.61 = f32[4,128,128]{1,2,0:T(8,128)S(1)} pad(f32[4,64,128]{1,2,0:T(8,128)S(1)} %add.195, f32[]{:T(128)} %constant.10.clone.1), padding=0_0_0x1_0_1x0_0_0 | pad | bytes 393220 | tf_op jit(solution)/shard_map/pad | solution.py:110
  281.2 4.5 %pad.60 = f32[4,128,128]{1,2,0:T(8,128)S(1)} pad(f32[4,64,128]{1,2,0:T(8,128)S(1)} %pad_maximum_fusion.2, f32[]{:T(128)} %constant.10.clone.1), padding=0_0_0x0_1_1x0_0_0 | pad | bytes 393220 | tf_op jit(solution)/shard_map/pad | solution.py:110
  287.3 7.7 %all-to-all-start.2 = ((bf16[8,512,128]{1,2,0:T(8,128)(2,1)}), bf16[8,512,128]{1,2,0:T(8,128)(2,1)S(1)}, u32[]{:S(2)}, u32[]{:S(2)}) async-start(bf16[8,512,128]{1,2,0:T(8,128)(2,1)} %broadcast_in_dim.10), calls=%async_computation.2 | async-start | bytes 2097152 | tf_op jit(solution)/shard_map/all_to_all | solution.py:15
  295.0 10.3 %all_gather.49 = bf16[128,256]{1,0:T(8,128)(2,1)S(1)} all-gather(bf16[32,256]{1,0:T(8,128)(2,1)S(1)} %convert_element_type.142), channel_id=1, replica_groups=mesh['fs_0'=8,'fs_1'=4,'tp'=8] {'fs_1'}, dimensions={0}, use_global_device_ids=true | all-gather | bytes 81920 | tf_op jit(solution)/shard_map/all_gather | solution.py:32
  305.3 20.3 %all_gather.50 = bf16[1024,256]{1,0:T(8,128)(2,1)S(1)} all-gather(bf16[128,256]{1,0:T(8,128)(2,1)S(1)} %all_gather.49), channel_id=1, replica_groups=mesh['fs_0'=8,'fs_1'=4,'tp'=8] {'fs_0'}, dimensions={0}, use_global_device_ids=true | all-gather | bytes 589824 | tf_op jit(solution)/shard_map/all_gather | solution.py:32
  328.3 12.1 %all-to-all-start.3 = ((bf16[8,512,256]{1,2,0:T(8,128)(2,1)}), bf16[8,512,256]{1,2,0:T(8,128)(2,1)S(1)}, u32[]{:S(2)}, u32[]{:S(2)}) async-start(bf16[8,512,256]{1,2,0:T(8,128)(2,1)} %broadcast_in_dim.11), calls=%async_computation.3 | async-start | bytes 4194304 | tf_op jit(solution)/shard_map/all_to_all | solution.py:15
  340.5 10.3 %all_gather.54 = bf16[352,256]{1,0:T(8,128)(2,1)} all-gather(bf16[88,256]{1,0:T(8,128)(2,1)S(1)} %convert_element_type.151), channel_id=1, replica_groups=mesh['fs_0'=8,'fs_1'=4,'tp'=8] {'fs_1'}, dimensions={0}, use_global_device_ids=true | all-gather | bytes 225280 | tf_op jit(solution)/shard_map/all_gather | solution.py:32
  350.9 15.8 %all-to-all-done.3 = bf16[8,512,256]{1,2,0:T(8,128)(2,1)S(1)} async-done(((bf16[8,512,256]{1,2,0:T(8,128)(2,1)}), bf16[8,512,256]{1,2,0:T(8,128)(2,1)S(1)}, u32[]{:S(2)}, u32[]{:S(2)}) %all-to-all-start.3) | async-done | bytes 2097184 | tf_op jit(solution)/shard_map/all_to_all | solution.py:15
  369.0 4.3 fusion.58
  374.3 11.7 %all-gather.20.cloned.1.call-done = bf16[2816,256]{1,0:T(8,128)(2,1)} async-done(((bf16[352,256]{1,0:T(8,128)(2,1)}), bf16[2816,256]{1,0:T(8,128)(2,1)}) %all-gather.20.cloned.1.call-update) | async-done | bytes 1441808 | tf_op jit(solution)/shard_map/all_gather | solution.py:32
  386.0 34.4 %all-gather.18.cloned.1.call-done = bf16[512,2816]{0,1:T(8,128)(2,1)} async-done(((bf16[512,352]{0,1:T(8,128)(2,1)}), bf16[512,2816]{0,1:T(8,128)(2,1)}) %all-gather.18.cloned.1.call-update) | async-done | bytes 2883600 | tf_op jit(solution)/shard_map/all_gather | solution.py:65
  420.4 3.9 fusion.11
  (187 shorter events, 87.9 us)
Async XLA Ops:
  6.5 63.8 %all-gather.8.cloned.1.call-start = ((), (), s32[]{:S(2)}) async-start(), calls=%async_computation.4 | async-start | bytes 3538944 | tf_op jit(solution)/shard_map/all_gather | solution.py:32
  23.4 8.2 %copy-start.9 = (f32[88,256]{1,0:T(8,128)S(1)}, f32[88,256]{1,0:T(8,128)}, u32[]{:S(2)}) copy-start(f32[88,256]{1,0:T(8,128)} %param.22) | copy-start | bytes 270340
  23.4 34.4 %all-to-all-start = ((bf16[8,512,256]{1,2,0:T(8,128)(2,1)}), bf16[8,512,256]{1,2,0:T(8,128)(2,1)S(1)}, u32[]{:S(2)}, u32[]{:S(2)}) async-start(bf16[8,512,256]{1,2,0:T(8,128)(2,1)} %broadcast_in_dim.8), calls=%async_computation | async-start | bytes 4194304 | tf_op jit(solution)/shard_map/all_to_all | solution.py:15
  31.5 26.8 %copy-start.14 = (f32[2048]{0:T(1024)S(1)}, f32[2048]{0:T(1024)}, u32[]{:S(2)}) copy-start(f32[2048]{0:T(1024)} %param.19) | copy-start | bytes 24580
  31.5 75.0 %all-gather.12.cloned.1.call-start = ((), (), s32[]{:S(2)}) async-start(), calls=%async_computation.6 | async-start | bytes 1622016 | tf_op jit(solution)/shard_map/all_gather | solution.py:32
  42.2 98.4 %all-gather.10.cloned.1.call-start = ((), (), s32[]{:S(2)}) async-start(), calls=%async_computation.5 | async-start | bytes 3244032 | tf_op jit(solution)/shard_map/all_gather | solution.py:65
  74.5 1.1 copy-start.11
  74.5 1.1 copy-start.12
  74.5 66.1 %copy-start.2 = (bf16[512,256]{1,0:T(8,128)(2,1)S(1)}, bf16[512,256]{1,0:T(8,128)(2,1)}, u32[]{:S(2)}) copy-start(bf16[512,256]{1,0:T(8,128)(2,1)} %param.18) | copy-start | bytes 786436
  75.5 102.5 %all-gather.14.cloned.1.call-start = ((), (), s32[]{:S(2)}) async-start(), calls=%async_computation.7 | async-start | bytes 1179648 | tf_op jit(solution)/shard_map/all_gather | solution.py:32
  143.8 1.7 copy-start.3
  145.4 4.0 copy-start.7
  145.4 4.0 copy-start.8
  145.4 15.2 %copy-start.21 = (f32[128]{0:T(128)S(1)}, f32[128]{0:T(128)}, u32[]{:S(2)}) copy-start(f32[128]{0:T(128)} %param.29) | copy-start | bytes 1540
  145.4 15.2 %copy-start.18 = (f32[4,128]{1,0:T(4,128)S(1)}, f32[4,128]{1,0:T(4,128)}, u32[]{:S(2)}) copy-start(f32[4,128]{1,0:T(4,128)} %param.26) | copy-start | bytes 6148
  145.5 30.2 %all-to-all-start.1 = ((bf16[8,512,256]{1,2,0:T(8,128)(2,1)}), bf16[8,512,256]{1,2,0:T(8,128)(2,1)S(1)}, u32[]{:S(2)}, u32[]{:S(2)}) async-start(bf16[8,512,256]{1,2,0:T(8,128)(2,1)} %broadcast_in_dim.9), calls=%async_computation.1 | async-start | bytes 4194304 | tf_op jit(solution)/shard_map/all_to_all | solution.py:15
  149.4 26.8 %copy-start.15 = (f32[2048]{0:T(1024)S(1)}, f32[2048]{0:T(1024)}, u32[]{:S(2)}) copy-start(f32[2048]{0:T(1024)} %param.23) | copy-start | bytes 24580
  149.4 219.7 %all-gather.16.cloned.1.call-start = ((), (), s32[]{:S(2)}) async-start(), calls=%async_computation.8 | async-start | bytes 3538944 | tf_op jit(solution)/shard_map/all_gather | solution.py:32
  178.0 3.9 copy-start.19
  180.6 1.6 copy-start.20
  262.5 7.2 %copy-start.5 = (f32[4,15,128]{1,2,0:T(8,128)S(1)}, f32[4,15,128]{1,2,0:T(8,128)}, u32[]{:S(2)}) copy-start(f32[4,15,128]{1,2,0:T(8,128)} %slice.222) | copy-start | bytes 92164
  262.6 7.2 %copy-start.6 = (f32[4,15,128]{1,2,0:T(8,128)S(1)}, f32[4,15,128]{1,2,0:T(8,128)}, u32[]{:S(2)}) copy-start(f32[4,15,128]{1,2,0:T(8,128)} %slice.255) | copy-start | bytes 92164
  281.0 4.9 %copy-start.1 = (f32[512,256]{1,0:T(8,128)S(1)}, f32[512,256]{1,0:T(8,128)}, u32[]{:S(2)}) copy-start(f32[512,256]{1,0:T(8,128)} %copy-done) | copy-start | bytes 1572868
  285.9 9.0 %copy-start.13 = (f32[32,256]{1,0:T(8,128)S(1)}, f32[32,256]{1,0:T(8,128)}, u32[]{:S(2)}) copy-start(f32[32,256]{1,0:T(8,128)} %param.31) | copy-start | bytes 98308
  287.3 38.6 %copy-start.17 = (f32[1024]{0:T(1024)S(1)}, f32[1024]{0:T(1024)}, u32[]{:S(2)}) copy-start(f32[1024]{0:T(1024)} %param.30) | copy-start | bytes 12292
  287.3 38.3 %all-to-all-start.2 = ((bf16[8,512,128]{1,2,0:T(8,128)(2,1)}), bf16[8,512,128]{1,2,0:T(8,128)(2,1)S(1)}, u32[]{:S(2)}, u32[]{:S(2)}) async-start(bf16[8,512,128]{1,2,0:T(8,128)(2,1)} %broadcast_in_dim.10), calls=%async_computation.2 | async-start | bytes 2097152 | tf_op jit(solution)/shard_map/all_to_all | solution.py:15
  295.0 31.2 %copy-start.4 = (bf16[512,256]{1,0:T(8,128)(2,1)S(1)}, bf16[512,256]{1,0:T(8,128)(2,1)}, u32[]{:S(2)}) copy-start(bf16[512,256]{1,0:T(8,128)(2,1)} %copy-done.3) | copy-start | bytes 786436
  328.3 12.1 %copy-start.10 = (f32[88,256]{1,0:T(8,128)S(1)}, f32[88,256]{1,0:T(8,128)}, u32[]{:S(2)}) copy-start(f32[88,256]{1,0:T(8,128)} %param.35) | copy-start | bytes 270340
  328.3 38.3 %all-to-all-start.3 = ((bf16[8,512,256]{1,2,0:T(8,128)(2,1)}), bf16[8,512,256]{1,2,0:T(8,128)(2,1)S(1)}, u32[]{:S(2)}, u32[]{:S(2)}) async-start(bf16[8,512,256]{1,2,0:T(8,128)(2,1)} %broadcast_in_dim.11), calls=%async_computation.3 | async-start | bytes 4194304 | tf_op jit(solution)/shard_map/all_to_all | solution.py:15
  340.4 26.7 %copy-start.16 = (f32[2048]{0:T(1024)S(1)}, f32[2048]{0:T(1024)}, u32[]{:S(2)}) copy-start(f32[2048]{0:T(1024)} %param.32) | copy-start | bytes 24580
  340.4 45.6 %all-gather.20.cloned.1.call-start = ((), (), s32[]{:S(2)}) async-start(), calls=%async_computation.10 | async-start | bytes 1622016 | tf_op jit(solution)/shard_map/all_gather | solution.py:32
  350.8 69.6 %all-gather.18.cloned.1.call-start = ((), (), s32[]{:S(2)}) async-start(), calls=%async_computation.9 | async-start | bytes 3244032 | tf_op jit(solution)/shard_map/all_gather | solution.py:65
  (1 other events, 0.8 us)
Sparse Core Ops, SparseCore 0:
  20.9 49.3 all-gather.7
  72.1 34.3 all-gather.11
  108.3 32.2 all-gather.9
  142.2 34.1 all-gather.13
  178.0 47.0 all-gather.15
  350.9 35.0 all-gather.19
  387.8 32.5 all-gather.17
where the time goes:
time: 439 us; the launch traced here: 431 us
  waiting for transfers between devices  157 us (36%)
  local copies, waits for them, and re-layouts  101 us (23%)
  blocking collectives  85.3 us (19%)
  starting transfers between devices  32 us (7%)
  other arithmetic  22 us (5%)
  matrix products  19.2 us (4%)
  between operations  14.6 us (3%)
    all_gather x7, blocking collectives, gathered_by_axis(): whole = lax.all_gather(whole, axes[number], axis=dim, tiled=True)  85.3 us
    all_gather x2, waiting for transfers between devices, feed_forward(): all_hidden = lax.all_gather(hidden, 'tp', axis=1, tiled=True)  68.5 us
    slice x34, local copies, waits for them, and re-layouts, recurrent_mixer(): lax.associative_scan(combine, (jnp.exp(log_keep), inject), axis=1)  65.6 us
    all_to_all x4, waiting for transfers between devices, copy_for_each(): return lax.all_to_all(copies, axis, split_axis=0, concat_axis=0, tiled=True)  46.2 us
    all_gather x5, waiting for transfers between devices, gathered_by_axis(): whole = lax.all_gather(whole, axes[number], axis=dim, tiled=True)  42.3 us
    all_to_all x4, starting transfers between devices, copy_for_each(): return lax.all_to_all(copies, axis, split_axis=0, concat_axis=0, tiled=True)  31.9 us
    pad x12, local copies, waits for them, and re-layouts, recurrent_mixer(): lax.associative_scan(combine, (jnp.exp(log_keep), inject), axis=1)  20.2 us
    dot_general x6, matrix products, contract(): jnp.dot(operand, gathered_by_axis(stacked.astype(jnp.bfloat16), FS, 0), p...  18.7 us
  transfers between devices with their start and end apart: 11, of which 8 were waited for; matrix products, arithmetic and copies ran while one was open for 31% of the time, Pallas kernels for 0%

commit v1 on v0

--- a/solution.py
+++ b/solution.py
@@ -8,6 +8,14 @@
 FS = ("fs_0", "fs_1")
 EPSILON = 1e-06
 DECAY_SCALE = 8.0
+
+
+def gather_by_exchange(shard, axis, dim):
+    size = lax.axis_size(axis)
+    repeats = [size if d == dim else 1 for d in range(shard.ndim)]
+    return lax.all_to_all(
+        jnp.tile(shard, repeats), axis, split_axis=dim, concat_axis=dim, tiled=True
+    )
 
 
 def copy_for_each(x, axis):
@@ -62,7 +70,7 @@
     products = contract(normed, jnp.concatenate((gate_matrix, up_matrix), axis=1))
     split_at = gate_matrix.shape[1]
     hidden = (jax.nn.silu(products[:, :split_at]) * products[:, split_at:]).astype(jnp.bfloat16)
-    all_hidden = lax.all_gather(hidden, "tp", axis=1, tiled=True)
+    all_hidden = gather_by_exchange(hidden, "tp", 1)
     return (residual.astype(jnp.float32) + 0.5 * contract(all_hidden, down_matrix)).astype(
         jnp.bfloat16
     )

time: 439 us -> 405 us (0.923)
  waiting for transfers between devices: 157 us -> 115 us
  starting transfers between devices: 32 us -> 40.1 us
    all_gather x2 -> x0, waiting for transfers between devices: 68.5 us -> none  [feed_forward(): all_hidden = lax.all_gather(hidden, 'tp', axis=1, tiled=True)]
    all_to_all x0 -> x2, waiting for transfers between devices: none -> 38.5 us  [gather_by_exchange(): lax.all_to_all(jnp.tile(shard, repeats), axis, split_axis=dim, concat_axi...]
    all_gather x5, waiting for transfers between devices: 42.3 us -> 30 us  [gathered_by_axis(): whole = lax.all_gather(whole, axes[number], axis=dim, tiled=True)]
    all_to_all x0 -> x2, starting transfers between devices: none -> 10.1 us  [gather_by_exchange(): lax.all_to_all(jnp.tile(shard, repeats), axis, split_axis=dim, concat_axi...]
  transfers between devices with their start and end apart: 11 -> 11, of which waited for: 8 -> 8; matrix products, arithmetic and copies ran while one was open for 31% -> 34% of each run, Pallas kernels for 0% -> 0%
where the time goes in v1:
time: 405 us; the launch traced here: 397 us
  waiting for transfers between devices  115 us (28%)
  local copies, waits for them, and re-layouts  105 us (26%)
  blocking collectives  85.5 us (21%)
  starting transfers between devices  40.1 us (10%)
  other arithmetic  20.5 us (5%)
  matrix products  17.5 us (4%)
  between operations  14.2 us (4%)
    all_gather x7, blocking collectives, gathered_by_axis(): whole = lax.all_gather(whole, axes[number], axis=dim, tiled=True)  85.5 us
    slice x34, local copies, waits for them, and re-layouts, recurrent_mixer(): lax.associative_scan(combine, (jnp.exp(log_keep), inject), axis=1)  65.6 us
    all_to_all x4, waiting for transfers between devices, copy_for_each(): return lax.all_to_all(copies, axis, split_axis=0, concat_axis=0, tiled=True)  46 us
    all_to_all x2, waiting for transfers between devices, gather_by_exchange(): lax.all_to_all(jnp.tile(shard, repeats), axis, split_axis=dim, concat_axi...  38.5 us
    all_gather x5, waiting for transfers between devices, gathered_by_axis(): whole = lax.all_gather(whole, axes[number], axis=dim, tiled=True)  30 us
    all_to_all x4, starting transfers between devices, copy_for_each(): return lax.all_to_all(copies, axis, split_axis=0, concat_axis=0, tiled=True)  30 us
    pad x12, local copies, waits for them, and re-layouts, recurrent_mixer(): lax.associative_scan(combine, (jnp.exp(log_keep), inject), axis=1)  20.2 us
    dot_general x6, matrix products, contract(): jnp.dot(operand, gathered_by_axis(stacked.astype(jnp.bfloat16), FS, 0), p...  16.9 us
  transfers between devices with their start and end apart: 11, of which 8 were waited for; matrix products, arithmetic and copies ran while one was open for 34% of the time, Pallas kernels for 0%

profile of v1, /device:TPU:1, one launch (start us, length us, event | category | flops | bytes accessed | tf_op | source)
XLA Modules:
  0.0 397.2 jit_solution(248016179326459989)
XLA Ops:
  8.4 12.3 %all_gather.36 = bf16[256,704]{1,0:T(8,128)(2,1)} all-gather(bf16[64,704]{1,0:T(8,128)(2,1)S(1)} %pad_maximum_fusion.3), channel_id=1, replica_groups=mesh['fs_0'=8,'fs_1'=4,'tp'=8] {'fs_1'}, dimensions={0}, use_global_device_ids=true | all-gather | bytes 450560 | tf_op jit(solution)/shard_map/all_gather | solution.py:40
  23.4 8.2 %all-to-all-start = ((bf16[8,512,256]{1,2,0:T(8,128)(2,1)}), bf16[8,512,256]{1,2,0:T(8,128)(2,1)S(1)}, u32[]{:S(2)}, u32[]{:S(2)}) async-start(bf16[8,512,256]{1,2,0:T(8,128)(2,1)} %broadcast_in_dim.8), calls=%async_computation | async-start | bytes 4194304 | tf_op jit(solution)/shard_map/all_to_all | solution.py:23
  31.5 10.6 %all_gather.38 = bf16[352,256]{1,0:T(8,128)(2,1)} all-gather(bf16[88,256]{1,0:T(8,128)(2,1)S(1)} %convert_element_type.124), channel_id=1, replica_groups=mesh['fs_0'=8,'fs_1'=4,'tp'=8] {'fs_1'}, dimensions={0}, use_global_device_ids=true | all-gather | bytes 225280 | tf_op jit(solution)/shard_map/all_gather | solution.py:40
  42.2 15.6 %all-to-all-done = bf16[8,512,256]{1,2,0:T(8,128)(2,1)S(1)} async-done(((bf16[8,512,256]{1,2,0:T(8,128)(2,1)}), bf16[8,512,256]{1,2,0:T(8,128)(2,1)S(1)}, u32[]{:S(2)}, u32[]{:S(2)}) %all-to-all-start) | async-done | bytes 2097184 | tf_op jit(solution)/shard_map/all_to_all | solution.py:23
  60.1 10.1 %all-gather.6.cloned.1.call-done = bf16[2048,704]{1,0:T(8,128)(2,1)} async-done(((bf16[256,704]{1,0:T(8,128)(2,1)}), bf16[2048,704]{1,0:T(8,128)(2,1)}) %all-gather.6.cloned.1.call-update) | async-done | bytes 2883600 | tf_op jit(solution)/shard_map/all_gather | solution.py:40
  70.3 4.2 %fusion.56 = f32[512,704]{0,1:T(8,128)S(1)} fusion(bf16[512,2048]{0,1:T(8,128)(2,1)} %fusion.5, bf16[2048,704]{1,0:T(8,128)(2,1)} %all-gather.6.cloned.1.call-done), kind=kOutput, calls=%fused_computation.110 | convolution fusion | flops 1476395008 | bytes 6422528 | tf_op jit(solution)/shard_map/dot_general | solution.py:61
  76.6 5.7 %all-to-all-start.1 = ((bf16[512,8,352]{0,2,1:T(8,128)(2,1)}), bf16[512,8,352]{0,2,1:T(8,128)(2,1)S(1)}, u32[]{:S(2)}, u32[]{:S(2)}) async-start(bf16[512,8,352]{0,2,1:T(8,128)(2,1)} %tile.4), calls=%async_computation.1 | async-start | bytes 5767168 | tf_op jit(solution)/shard_map/all_to_all | solution.py:16
  82.3 10.8 %all_gather.40 = bf16[256,256]{1,0:T(8,128)(2,1)} all-gather(bf16[64,256]{1,0:T(8,128)(2,1)S(1)} %pad_maximum_fusion.5), channel_id=1, replica_groups=mesh['fs_0'=8,'fs_1'=4,'tp'=8] {'fs_1'}, dimensions={0}, use_global_device_ids=true | all-gather | bytes 163840 | tf_op jit(solution)/shard_map/all_gather | solution.py:40
  93.1 13.5 %all-gather.8.cloned.1.call-done = bf16[2816,256]{1,0:T(8,128)(2,1)} async-done(((bf16[352,256]{1,0:T(8,128)(2,1)}), bf16[2816,256]{1,0:T(8,128)(2,1)}) %all-gather.8.cloned.1.call-update) | async-done | bytes 1441808 | tf_op jit(solution)/shard_map/all_gather | solution.py:40
  106.6 10.3 %all-to-all-done.1 = bf16[512,8,352]{0,2,1:T(8,128)(2,1)S(1)} async-done(((bf16[512,8,352]{0,2,1:T(8,128)(2,1)}), bf16[512,8,352]{0,2,1:T(8,128)(2,1)S(1)}, u32[]{:S(2)}, u32[]{:S(2)}) %all-to-all-start.1) | async-done | bytes 2883616 | tf_op jit(solution)/shard_map/all_to_all | solution.py:16
  120.9 4.6 %all-to-all-start.2 = ((bf16[8,512,256]{1,2,0:T(8,128)(2,1)}), bf16[8,512,256]{1,2,0:T(8,128)(2,1)S(1)}, u32[]{:S(2)}, u32[]{:S(2)}) async-start(bf16[8,512,256]{1,2,0:T(8,128)(2,1)} %broadcast_in_dim.9), calls=%async_computation.2 | async-start | bytes 4194304 | tf_op jit(solution)/shard_map/all_to_all | solution.py:23
  125.6 11.4 %all_gather.44 = bf16[256,704]{1,0:T(8,128)(2,1)} all-gather(bf16[64,704]{1,0:T(8,128)(2,1)S(1)} %pad_maximum_fusion.4), channel_id=1, replica_groups=mesh['fs_0'=8,'fs_1'=4,'tp'=8] {'fs_1'}, dimensions={0}, use_global_device_ids=true | all-gather | bytes 450560 | tf_op jit(solution)/shard_map/all_gather | solution.py:40
  137.1 14.6 %all-to-all-done.2 = bf16[8,512,256]{1,2,0:T(8,128)(2,1)S(1)} async-done(((bf16[8,512,256]{1,2,0:T(8,128)(2,1)}), bf16[8,512,256]{1,2,0:T(8,128)(2,1)S(1)}, u32[]{:S(2)}, u32[]{:S(2)}) %all-to-all-start.2) | async-done | bytes 2097184 | tf_op jit(solution)/shard_map/all_to_all | solution.py:23
  159.0 4.9 %slice.212 = f32[4,64,128]{1,2,0:T(8,128)S(1)} slice(f32[4,128,128]{1,2,0:T(8,128)S(1)} %get-tuple-element.6), slice={[0:4:1], [0:127:2], [0:128:1]} | slice | bytes 262144 | tf_op jit(solution)/shard_map/slice | solution.py:118
  164.0 4.5 %slice.213 = f32[4,64,128]{1,2,0:T(8,128)S(1)} slice(f32[4,128,128]{1,2,0:T(8,128)S(1)} %get-tuple-element.6), slice={[0:4:1], [1:128:2], [0:128:1]} | slice | bytes 262144 | tf_op jit(solution)/shard_map/slice | solution.py:118
  168.5 4.5 %slice.211 = f32[4,64,128]{1,2,0:T(8,128)S(1)} slice(f32[4,128,128]{1,2,0:T(8,128)S(1)} %get-tuple-element.5), slice={[0:4:1], [1:128:2], [0:128:1]} | slice | bytes 262144 | tf_op jit(solution)/shard_map/slice | solution.py:118
  173.1 4.5 %slice.215 = f32[4,64,128]{1,2,0:T(8,128)S(1)} slice(f32[4,128,128]{1,2,0:T(8,128)S(1)} %get-tuple-element.5), slice={[0:4:1], [0:127:2], [0:128:1]} | slice | bytes 262144 | tf_op jit(solution)/shard_map/slice | solution.py:118
  221.7 4.5 %slice.259 = f32[4,63,128]{1,2,0:T(8,128)S(1)} slice(f32[4,128,128]{1,2,0:T(8,128)S(1)} %get-tuple-element.6), slice={[0:4:1], [2:128:2], [0:128:1]} | slice | bytes 258048 | tf_op jit(solution)/shard_map/slice | solution.py:118
  226.2 4.5 %slice.210 = f32[4,63,128]{1,2,0:T(8,128)S(1)} slice(f32[4,128,128]{1,2,0:T(8,128)S(1)} %get-tuple-element.5), slice={[0:4:1], [2:128:2], [0:128:1]} | slice | bytes 258048 | tf_op jit(solution)/shard_map/slice | solution.py:118
  252.5 4.6 %pad.61 = f32[4,128,128]{1,2,0:T(8,128)S(1)} pad(f32[4,64,128]{1,2,0:T(8,128)S(1)} %add.195, f32[]{:T(128)} %constant.10.clone.1), padding=0_0_0x1_0_1x0_0_0 | pad | bytes 393220 | tf_op jit(solution)/shard_map/pad | solution.py:118
  257.3 4.5 %pad.60 = f32[4,128,128]{1,2,0:T(8,128)S(1)} pad(f32[4,64,128]{1,2,0:T(8,128)S(1)} %pad_maximum_fusion.2, f32[]{:T(128)} %constant.10.clone.1), padding=0_0_0x0_1_1x0_0_0 | pad | bytes 393220 | tf_op jit(solution)/shard_map/pad | solution.py:118
  263.4 4.6 %all-to-all-start.3 = ((bf16[8,512,128]{1,2,0:T(8,128)(2,1)}), bf16[8,512,128]{1,2,0:T(8,128)(2,1)S(1)}, u32[]{:S(2)}, u32[]{:S(2)}) async-start(bf16[8,512,128]{1,2,0:T(8,128)(2,1)} %broadcast_in_dim.10), calls=%async_computation.3 | async-start | bytes 2097152 | tf_op jit(solution)/shard_map/all_to_all | solution.py:23
  267.9 10.3 %all_gather.42 = bf16[128,256]{1,0:T(8,128)(2,1)S(1)} all-gather(bf16[32,256]{1,0:T(8,128)(2,1)S(1)} %convert_element_type.142), channel_id=1, replica_groups=mesh['fs_0'=8,'fs_1'=4,'tp'=8] {'fs_1'}, dimensions={0}, use_global_device_ids=true | all-gather | bytes 81920 | tf_op jit(solution)/shard_map/all_gather | solution.py:40
  278.2 19.7 %all_gather.43 = bf16[1024,256]{1,0:T(8,128)(2,1)S(1)} all-gather(bf16[128,256]{1,0:T(8,128)(2,1)S(1)} %all_gather.42), channel_id=1, replica_groups=mesh['fs_0'=8,'fs_1'=4,'tp'=8] {'fs_0'}, dimensions={0}, use_global_device_ids=true | all-gather | bytes 589824 | tf_op jit(solution)/shard_map/all_gather | solution.py:40
  300.7 12.7 %all-to-all-start.4 = ((bf16[8,512,256]{1,2,0:T(8,128)(2,1)}), bf16[8,512,256]{1,2,0:T(8,128)(2,1)S(1)}, u32[]{:S(2)}, u32[]{:S(2)}) async-start(bf16[8,512,256]{1,2,0:T(8,128)(2,1)} %broadcast_in_dim.11), calls=%async_computation.4 | async-start | bytes 4194304 | tf_op jit(solution)/shard_map/all_to_all | solution.py:23
  313.4 10.3 %all_gather.46 = bf16[352,256]{1,0:T(8,128)(2,1)} all-gather(bf16[88,256]{1,0:T(8,128)(2,1)S(1)} %convert_element_type.151), channel_id=1, replica_groups=mesh['fs_0'=8,'fs_1'=4,'tp'=8] {'fs_1'}, dimensions={0}, use_global_device_ids=true | all-gather | bytes 225280 | tf_op jit(solution)/shard_map/all_gather | solution.py:40
  323.8 15.8 %all-to-all-done.4 = bf16[8,512,256]{1,2,0:T(8,128)(2,1)S(1)} async-done(((bf16[8,512,256]{1,2,0:T(8,128)(2,1)}), bf16[8,512,256]{1,2,0:T(8,128)(2,1)S(1)}, u32[]{:S(2)}, u32[]{:S(2)}) %all-to-all-start.4) | async-done | bytes 2097184 | tf_op jit(solution)/shard_map/all_to_all | solution.py:23
  342.0 4.3 %fusion.58 = f32[512,704]{0,1:T(8,128)S(1)} fusion(bf16[512,2048]{0,1:T(8,128)(2,1)} %fusion.1, bf16[2048,704]{1,0:T(8,128)(2,1)} %all-gather.12.cloned.1.call-done), kind=kOutput, calls=%fused_computation.112 | convolution fusion | flops 1476395008 | bytes 6422528 | tf_op jit(solution)/shard_map/dot_general | solution.py:61
  348.3 4.5 %all-to-all-start.5 = ((bf16[512,8,352]{0,2,1:T(8,128)(2,1)}), bf16[512,8,352]{0,2,1:T(8,128)(2,1)S(1)}, u32[]{:S(2)}, u32[]{:S(2)}) async-start(bf16[512,8,352]{0,2,1:T(8,128)(2,1)} %tile.5), calls=%async_computation.5 | async-start | bytes 5767168 | tf_op jit(solution)/shard_map/all_to_all | solution.py:16
  352.7 6.4 %all-gather.14.cloned.1.call-done = bf16[2816,256]{1,0:T(8,128)(2,1)} async-done(((bf16[352,256]{1,0:T(8,128)(2,1)}), bf16[2816,256]{1,0:T(8,128)(2,1)}) %all-gather.14.cloned.1.call-update) | async-done | bytes 1441808 | tf_op jit(solution)/shard_map/all_gather | solution.py:40
  359.1 28.2 %all-to-all-done.5 = bf16[512,8,352]{0,2,1:T(8,128)(2,1)S(1)} async-done(((bf16[512,8,352]{0,2,1:T(8,128)(2,1)}), bf16[512,8,352]{0,2,1:T(8,128)(2,1)S(1)}, u32[]{:S(2)}, u32[]{:S(2)}) %all-to-all-start.5) | async-done | bytes 2883616 | tf_op jit(solution)/shard_map/all_to_all | solution.py:16
  387.4 3.0 fusion.11
  (187 shorter events, 94.8 us)
Async XLA Ops:
  6.5 63.8 %all-gather.6.cloned.1.call-start = ((), (), s32[]{:S(2)}) async-start(), calls=%async_computation.6 | async-start | bytes 3538944 | tf_op jit(solution)/shard_map/all_gather | solution.py:40
  23.4 8.2 %copy-start.9 = (f32[88,256]{1,0:T(8,128)S(1)}, f32[88,256]{1,0:T(8,128)}, u32[]{:S(2)}) copy-start(f32[88,256]{1,0:T(8,128)} %param.22) | copy-start | bytes 270340
  23.4 34.4 %all-to-all-start = ((bf16[8,512,256]{1,2,0:T(8,128)(2,1)}), bf16[8,512,256]{1,2,0:T(8,128)(2,1)S(1)}, u32[]{:S(2)}, u32[]{:S(2)}) async-start(bf16[8,512,256]{1,2,0:T(8,128)(2,1)} %broadcast_in_dim.8), calls=%async_computation | async-start | bytes 4194304 | tf_op jit(solution)/shard_map/all_to_all | solution.py:23
  31.5 26.8 %copy-start.14 = (f32[2048]{0:T(1024)S(1)}, f32[2048]{0:T(1024)}, u32[]{:S(2)}) copy-start(f32[2048]{0:T(1024)} %param.19) | copy-start | bytes 24580
  31.5 75.1 %all-gather.8.cloned.1.call-start = ((), (), s32[]{:S(2)}) async-start(), calls=%async_computation.7 | async-start | bytes 1622016 | tf_op jit(solution)/shard_map/all_gather | solution.py:40
  76.6 5.7 %copy-start.11 = (f32[64,128]{1,0:T(8,128)S(1)}, f32[64,128]{1,0:T(8,128)}, u32[]{:S(2)}) copy-start(f32[64,128]{1,0:T(8,128)} %param.24) | copy-start | bytes 98308
  76.6 5.7 %copy-start.12 = (f32[64,128]{1,0:T(8,128)S(1)}, f32[64,128]{1,0:T(8,128)}, u32[]{:S(2)}) copy-start(f32[64,128]{1,0:T(8,128)} %param.25) | copy-start | bytes 98308
  76.6 40.3 %copy-start.2 = (bf16[512,256]{1,0:T(8,128)(2,1)S(1)}, bf16[512,256]{1,0:T(8,128)(2,1)}, u32[]{:S(2)}) copy-start(bf16[512,256]{1,0:T(8,128)(2,1)} %param.18) | copy-start | bytes 786436
  76.6 40.3 %all-to-all-start.1 = ((bf16[512,8,352]{0,2,1:T(8,128)(2,1)}), bf16[512,8,352]{0,2,1:T(8,128)(2,1)S(1)}, u32[]{:S(2)}, u32[]{:S(2)}) async-start(bf16[512,8,352]{0,2,1:T(8,128)(2,1)} %tile.4), calls=%async_computation.1 | async-start | bytes 5767168 | tf_op jit(solution)/shard_map/all_to_all | solution.py:16
  82.2 71.9 %all-gather.10.cloned.1.call-start = ((), (), s32[]{:S(2)}) async-start(), calls=%async_computation.8 | async-start | bytes 1179648 | tf_op jit(solution)/shard_map/all_gather | solution.py:40
  119.2 1.7 copy-start.3
  120.8 4.6 %copy-start.7 = (f32[64,352]{1,0:T(8,128)S(1)}, f32[64,352]{1,0:T(8,128)}, u32[]{:S(2)}) copy-start(f32[64,352]{1,0:T(8,128)} %param.33) | copy-start | bytes 270340
  120.8 4.7 %copy-start.8 = (f32[64,352]{1,0:T(8,128)S(1)}, f32[64,352]{1,0:T(8,128)}, u32[]{:S(2)}) copy-start(f32[64,352]{1,0:T(8,128)} %param.34) | copy-start | bytes 270340
  120.8 16.2 %copy-start.21 = (f32[128]{0:T(128)S(1)}, f32[128]{0:T(128)}, u32[]{:S(2)}) copy-start(f32[128]{0:T(128)} %param.29) | copy-start | bytes 1540
  120.8 16.3 %copy-start.18 = (f32[4,128]{1,0:T(4,128)S(1)}, f32[4,128]{1,0:T(4,128)}, u32[]{:S(2)}) copy-start(f32[4,128]{1,0:T(4,128)} %param.26) | copy-start | bytes 6148
  120.9 30.9 %all-to-all-start.2 = ((bf16[8,512,256]{1,2,0:T(8,128)(2,1)}), bf16[8,512,256]{1,2,0:T(8,128)(2,1)S(1)}, u32[]{:S(2)}, u32[]{:S(2)}) async-start(bf16[8,512,256]{1,2,0:T(8,128)(2,1)} %broadcast_in_dim.9), calls=%async_computation.2 | async-start | bytes 4194304 | tf_op jit(solution)/shard_map/all_to_all | solution.py:23
  125.5 26.8 %copy-start.15 = (f32[2048]{0:T(1024)S(1)}, f32[2048]{0:T(1024)}, u32[]{:S(2)}) copy-start(f32[2048]{0:T(1024)} %param.23) | copy-start | bytes 24580
  125.5 216.5 %all-gather.12.cloned.1.call-start = ((), (), s32[]{:S(2)}) async-start(), calls=%async_computation.9 | async-start | bytes 3538944 | tf_op jit(solution)/shard_map/all_gather | solution.py:40
  154.1 3.9 copy-start.19
  156.8 1.6 copy-start.20
  238.7 7.2 %copy-start.5 = (f32[4,15,128]{1,2,0:T(8,128)S(1)}, f32[4,15,128]{1,2,0:T(8,128)}, u32[]{:S(2)}) copy-start(f32[4,15,128]{1,2,0:T(8,128)} %slice.222) | copy-start | bytes 92164
  238.7 7.2 %copy-start.6 = (f32[4,15,128]{1,2,0:T(8,128)S(1)}, f32[4,15,128]{1,2,0:T(8,128)}, u32[]{:S(2)}) copy-start(f32[4,15,128]{1,2,0:T(8,128)} %slice.255) | copy-start | bytes 92164
  257.1 4.9 %copy-start.1 = (f32[512,256]{1,0:T(8,128)S(1)}, f32[512,256]{1,0:T(8,128)}, u32[]{:S(2)}) copy-start(f32[512,256]{1,0:T(8,128)} %copy-done) | copy-start | bytes 1572868
  262.0 5.9 %copy-start.13 = (f32[32,256]{1,0:T(8,128)S(1)}, f32[32,256]{1,0:T(8,128)}, u32[]{:S(2)}) copy-start(f32[32,256]{1,0:T(8,128)} %param.31) | copy-start | bytes 98308
  263.4 34.9 %copy-start.17 = (f32[1024]{0:T(1024)S(1)}, f32[1024]{0:T(1024)}, u32[]{:S(2)}) copy-start(f32[1024]{0:T(1024)} %param.30) | copy-start | bytes 12292
  263.4 34.6 %all-to-all-start.3 = ((bf16[8,512,128]{1,2,0:T(8,128)(2,1)}), bf16[8,512,128]{1,2,0:T(8,128)(2,1)S(1)}, u32[]{:S(2)}, u32[]{:S(2)}) async-start(bf16[8,512,128]{1,2,0:T(8,128)(2,1)} %broadcast_in_dim.10), calls=%async_computation.3 | async-start | bytes 2097152 | tf_op jit(solution)/shard_map/all_to_all | solution.py:23
  267.9 30.6 %copy-start.4 = (bf16[512,256]{1,0:T(8,128)(2,1)S(1)}, bf16[512,256]{1,0:T(8,128)(2,1)}, u32[]{:S(2)}) copy-start(bf16[512,256]{1,0:T(8,128)(2,1)} %copy-done.3) | copy-start | bytes 786436
  300.7 12.7 %copy-start.10 = (f32[88,256]{1,0:T(8,128)S(1)}, f32[88,256]{1,0:T(8,128)}, u32[]{:S(2)}) copy-start(f32[88,256]{1,0:T(8,128)} %param.35) | copy-start | bytes 270340
  300.7 38.9 %all-to-all-start.4 = ((bf16[8,512,256]{1,2,0:T(8,128)(2,1)}), bf16[8,512,256]{1,2,0:T(8,128)(2,1)S(1)}, u32[]{:S(2)}, u32[]{:S(2)}) async-start(bf16[8,512,256]{1,2,0:T(8,128)(2,1)} %broadcast_in_dim.11), calls=%async_computation.4 | async-start | bytes 4194304 | tf_op jit(solution)/shard_map/all_to_all | solution.py:23
  313.4 26.7 %copy-start.16 = (f32[2048]{0:T(1024)S(1)}, f32[2048]{0:T(1024)}, u32[]{:S(2)}) copy-start(f32[2048]{0:T(1024)} %param.32) | copy-start | bytes 24580
  313.4 45.8 %all-gather.14.cloned.1.call-start = ((), (), s32[]{:S(2)}) async-start(), calls=%async_computation.10 | async-start | bytes 1622016 | tf_op jit(solution)/shard_map/all_gather | solution.py:40
  348.3 39.1 %all-to-all-start.5 = ((bf16[512,8,352]{0,2,1:T(8,128)(2,1)}), bf16[512,8,352]{0,2,1:T(8,128)(2,1)S(1)}, u32[]{:S(2)}, u32[]{:S(2)}) async-start(bf16[512,8,352]{0,2,1:T(8,128)(2,1)} %tile.5), calls=%async_computation.5 | async-start | bytes 5767168 | tf_op jit(solution)/shard_map/all_to_all | solution.py:16
  (1 other events, 0.8 us)
Sparse Core Ops, SparseCore 0:
  20.9 49.3 all-gather.5
  72.1 34.4 all-gather.7
  108.4 36.5 all-gather.9
  146.7 47.1 all-gather.11
  323.9 35.2 all-gather.13
